TPU v7x, 32 devices: a whole 2x2x4 slice. The times are simulated.
32 devices in a mesh: grp: 2 (over y), ep: 4 (over z), tp: 4 (over x, core).
Axes of the slice: x: 2, y: 2, z: 4, core: 2. Of those that a mesh axis runs over, the one named last changes fastest.
Arguments:
- queries: bfloat16 [1024, 1024], P(('grp', 'ep'), 'tp'), parts along dimension 0, may hold values from -6 to 6
- keys: bfloat16 [1024, 1024], P(('grp', 'ep'), 'tp'), parts along dimension 0, may hold values from -6 to 6
- values: bfloat16 [1024, 1024], P(('grp', 'ep'), 'tp'), parts along dimension 0, may hold values from -6 to 6
- lambdas: float32 [8], P('tp'), may hold values from 0.3 to 0.8
- head_gain: float32 [128], replicated, may hold values from 0.1 to 1.9
- tokens: bfloat16 [2048, 1536], P(('grp', 'ep')), parts along dimension 0, may hold values from -6 to 6
- route_ids: int32 [2048, 2], P(('grp', 'ep')), parts along dimension 0, may hold values from 0 to 3, all different within a row; in each aligned block of 256 rows (0 to 255, 256 to 511, ...) at most 256 rows name the same one
- route_weights: float32 [2048, 2], P(('grp', 'ep')), parts along dimension 0, may hold values from 0.2 to 1
- moe_gain: float32 [1536], replicated, may hold values from 0.1 to 1.9
- w_gate: bfloat16 [4, 1536, 3072], P('ep', None, 'tp'), may hold values from -0.15625 to 0.15625
- w_up: bfloat16 [4, 1536, 3072], P('ep', None, 'tp'), may hold values from -0.15625 to 0.15625
- w_down: bfloat16 [4, 3072, 1536], P('ep', 'tp'), may hold values from -0.109375 to 0.109375
Outputs:
- heads_out: bfloat16 [1024, 1024], P(('grp', 'ep'), 'tp'), parts along dimension 0
- expert_out: bfloat16 [2048, 1536], P(('grp', 'ep'), 'tp'), parts along dimension 0
There are 2 independent parts, one for each index of `grp`. A program takes and returns all parts, laid end to end along the dimension named above; an argument that names none is the same for every part. Nothing has to cross between parts.
Inputs may be any that keep to these rules, and one draw needn't show every extreme that they name: `route_ids`: each row names 2 different experts. In the 256 rows of one device no expert is named more than 256 times, and in every draw some device names some expert exactly 256 times.
All inputs are finite; a program needn't handle non-finite values.
Results may differ from a plain program's by a relative error of at most 0.015.
Values may be sent and summed in bfloat16 or wider, within the bound.
A program may use at most 64 MiB of HBM per device.

v0:
```python
import jax
import jax.numpy as jnp
from jax import lax
from jax.sharding import PartitionSpec as P


def attend(queries, keys, values, lambdas, head_gain):
    row_count = queries.shape[0]
    head_count = lambdas.shape[0]
    head_dim = queries.shape[1] // (2 * head_count)
    value_dim = values.shape[1] // head_count
    query_parts = queries.reshape(row_count, head_count, 2, head_dim)
    score_scale = head_dim ** (-0.5)
    running = jnp.full((head_count, 2, row_count), -1e30, jnp.float32)
    key_piece = lax.all_gather(keys, "ep", axis=0, tiled=True)
    value_piece = lax.all_gather(values, "ep", axis=0, tiled=True)
    count = key_piece.shape[0]
    key_parts = key_piece.reshape(count, head_count, 2, head_dim)
    value_parts = value_piece.reshape(count, head_count, value_dim)
    scores = (
        jnp.einsum("qhcd,khcd->hcqk", query_parts, key_parts, preferred_element_type=jnp.float32)
        * score_scale
    )
    newest = jnp.maximum(running, jnp.max(scores, axis=-1))
    weights_now = jnp.exp(scores - newest[..., None])
    totals = jnp.sum(weights_now, axis=-1)
    sums = jnp.einsum(
        "hcqk,khe->hcqe",
        weights_now.astype(jnp.bfloat16),
        value_parts,
        preferred_element_type=jnp.float32,
    )
    running, totals, sums = (newest, totals, sums)
    means = sums / totals[..., None]
    mixed = means[:, 0] - lambdas[:, None, None] * means[:, 1]
    scaled = mixed * lax.rsqrt(jnp.mean(mixed * mixed, axis=-1, keepdims=True) + 1e-06) * head_gain
    return (
        jnp.transpose(scaled, (1, 0, 2))
        .reshape(row_count, head_count * value_dim)
        .astype(jnp.bfloat16)
    )


def experts(tokens, route_ids, route_weights, moe_gain, w_gate, w_up, w_down):
    row_count, width = tokens.shape
    top_count = route_ids.shape[1]
    ep_size = lax.axis_size("ep")
    tp_size = lax.axis_size("tp")
    expert_count = w_gate.shape[0] * ep_size
    capacity = 2 * row_count * top_count // expert_count
    token_float = tokens.astype(jnp.float32)
    normed = (
        token_float
        * lax.rsqrt(jnp.mean(token_float * token_float, axis=1, keepdims=True) + 1e-06)
        * moe_gain
    ).astype(jnp.bfloat16)
    flat_ids = route_ids.reshape(-1)
    onehot = (flat_ids[:, None] == jnp.arange(expert_count, dtype=jnp.int32)[None, :]).astype(
        jnp.int32
    )
    earlier = jnp.cumsum(onehot, axis=0) - onehot
    position = jnp.sum(earlier * onehot, axis=1)
    slot_index = flat_ids * capacity + position
    owners = (
        jnp.full((expert_count * capacity,), row_count, jnp.int32)
        .at[slot_index]
        .set(jnp.arange(row_count * top_count, dtype=jnp.int32) // top_count)
    )
    padded = jnp.concatenate([normed, jnp.zeros((1, width), jnp.bfloat16)], axis=0)
    outgoing = padded[owners].reshape(expert_count, capacity, width)
    gate_mat = w_gate[0]
    up_mat = w_up[0]
    down_mat = w_down[0]
    slice_width = width // tp_size
    own_columns = lax.dynamic_slice_in_dim(
        outgoing, lax.axis_index("tp") * slice_width, slice_width, 2
    )
    arrived = lax.all_to_all(own_columns, "ep", split_axis=0, concat_axis=0, tiled=True)
    piece = lax.all_gather(arrived, "tp", axis=2, tiled=True)
    gate = jnp.einsum("scd,df->scf", piece, gate_mat, preferred_element_type=jnp.float32)
    upward = jnp.einsum("scd,df->scf", piece, up_mat, preferred_element_type=jnp.float32)
    hidden = (jax.nn.silu(gate) * upward).astype(jnp.bfloat16)
    flat_hidden = hidden.reshape(-1, hidden.shape[2])
    summed = lax.psum_scatter(
        jnp.einsum("fd,sf->ds", down_mat, flat_hidden, preferred_element_type=jnp.float32).astype(
            jnp.bfloat16
        ),
        "tp",
        scatter_dimension=0,
        tiled=True,
    )
    back = lax.all_to_all(summed, "ep", split_axis=1, concat_axis=1, tiled=True)
    picked = (
        jnp.take(back, slot_index, axis=1).astype(jnp.float32).reshape(-1, row_count, top_count)
    )
    combined = jnp.einsum("drk,rk->rd", picked, route_weights)
    return combined.astype(jnp.bfloat16)


def on_device(
    queries,
    keys,
    values,
    lambdas,
    head_gain,
    tokens,
    route_ids,
    route_weights,
    moe_gain,
    w_gate,
    w_up,
    w_down,
):
    heads_out = attend(queries, keys, values, lambdas, head_gain)
    expert_out = experts(tokens, route_ids, route_weights, moe_gain, w_gate, w_up, w_down)
    return (heads_out, expert_out)


def solution(mesh):
    in_specs = (
        P(("grp", "ep"), "tp"),
        P(("grp", "ep"), "tp"),
        P(("grp", "ep"), "tp"),
        P("tp"),
        P(),
        P(("grp", "ep"), None),
        P(("grp", "ep"), None),
        P(("grp", "ep"), None),
        P(),
        P("ep", None, "tp"),
        P("ep", None, "tp"),
        P("ep", "tp", None),
    )
    out_specs = (P(("grp", "ep"), "tp"), P(("grp", "ep"), "tp"))
    return jax.shard_map(
        on_device, mesh=mesh, in_specs=in_specs, out_specs=out_specs, check_vma=False
    )
```

profile of v0, /device:TPU:0, one launch (start us, length us, event | category | flops | bytes accessed | tf_op | source)
XLA Modules:
  0.0 183.2 jit_solution(15858981580019613275)
XLA Ops:
  7.2 0.0 all-gather.2.cloned.1.call-start
  7.2 1.0 copy.40
  8.2 0.1 eq.26
  8.3 0.1 reshape.111
  8.5 0.7 broadcast_multiply_fusion
  9.2 1.2 reduce-window.6
  10.4 0.2 slice_reduce_fusion
  10.6 0.2 reduce-window.9
  10.8 0.1 add_bitcast_fusion
  10.9 0.1 copy.44
  11.0 0.1 mul.101
  11.2 2.4 %scatter_custom_fusion = s32[1024]{0:T(1024)S(1)} fusion(s32[512]{0:T(512)S(1)} %bitcast.95, s32[512]{0:T(512)S(1)} %add_select_fusion, s32[]{:T(128)} %constant.33.clone.1), kind=kCustom, calls=%fused_computation.53 | custom fusion | bytes 4100 | tf_op jit(solution)/shard_map/scatter | solution.py:67
  13.7 1.4 fusion.8
  15.1 1.4 fusion.10
  16.4 0.1 concatenate.3
  16.5 5.6 %gather_fusion = bf16[1024,1536]{1,0:T(8,128)(2,1)} fusion(bf16[257,1536]{1,0:T(8,128)(2,1)S(1)} %concatenate.3, s32[1024]{0:T(1024)S(1)} %fusion.23), kind=kCustom, calls=%fused_computation | custom fusion | bytes 6295552 | tf_op jit(solution)/shard_map/gather | solution.py:70
  22.1 1.2 constant_dynamic-slice_fusion
  23.3 26.4 %all_to_all.17 = bf16[4,256,384]{2,1,0:T(8,128)(2,1)} all-to-all(bf16[4,256,384]{2,1,0:T(8,128)(2,1)S(1)} %constant_dynamic-slice_fusion), channel_id=1, replica_groups=mesh['grp'=2,'ep'=4,'tp'=4] {'ep'}, dimensions={0} | all-to-all | bytes 1572864 | tf_op jit(solution)/shard_map/all_to_all | solution.py:78
  49.7 0.0 all-gather.2.cloned.1.call-update
  49.7 0.0 reduce-scatter.4.cloned.1.call-start
  49.8 27.7 %all-gather.2.cloned.1.call-done = bf16[4,256,1536]{2,1,0:T(8,128)(2,1)} async-done(((bf16[4,256,384]{2,1,0:T(8,128)(2,1)}), bf16[4,256,1536]{2,1,0:T(8,128)(2,1)}) %all-gather.2.cloned.1.call-update) | async-done | bytes 3145744 | tf_op jit(solution)/shard_map/all_gather | solution.py:79
  77.5 5.4 %fusion.2 = f32[4,256,768]{2,1,0:T(8,128)S(1)} fusion(bf16[4,256,1536]{2,1,0:T(8,128)(2,1)} %all-gather.2.cloned.1.call-done, bf16[1,1536,768]{2,1,0:T(8,128)(2,1)} %param.22), kind=kOutput, calls=%fused_computation.7 | convolution fusion | flops 2415919104 | bytes 8650752 | tf_op jit(solution)/shard_map/scd,df->scf/dot_general | solution.py:81
  82.8 2.9 %multiply_convert_fusion = bf16[4,256,768]{2,1,0:T(8,128)(2,1)S(1)} fusion(f32[4,256,768]{2,1,0:T(8,128)S(1)} %fusion.2, bf16[4,256,1536]{2,1,0:T(8,128)(2,1)S(1)} %copy-done.8, bf16[1,1536,768]{2,1,0:T(8,128)(2,1)S(1)} %copy-done.9), kind=kOutput, calls=%fused_computation.5 | convolution fusion | flops 2420637696 | bytes 10223616 | tf_op jit(solution)/shard_map/scd,df->scf/dot_general | solution.py:80
  85.8 4.0 %fusion = bf16[1536,1024]{0,1:T(8,128)(2,1)} fusion(bf16[1024,768]{1,0:T(8,128)(2,1)S(1)} %bitcast.99, bf16[1,768,1536]{2,1,0:T(8,128)(2,1)S(1)} %copy-done), kind=kOutput, calls=%fused_computation.4 | convolution fusion | flops 2417491968 | bytes 7077888 | tf_op jit(solution)/shard_map/fd,sf->ds/dot_general | solution.py:85
  89.8 4.6 %copy.49 = bf16[1536,1024]{1,0:T(8,128)(2,1)} copy(bf16[1536,1024]{0,1:T(8,128)(2,1)} %fusion) | data formatting | bytes 6291456
  94.5 0.1 reduce_sum.43
  94.6 0.1 copy.42
  94.7 0.4 copy-done.4
  95.1 0.8 copy.43
  95.9 0.8 copy.47
  96.7 13.9 %all_gather.9 = bf16[512,256]{1,0:T(8,128)(2,1)S(1)} all-gather(bf16[128,256]{1,0:T(8,128)(2,1)S(1)} %copy-done.1), channel_id=1, replica_groups=mesh['grp'=2,'ep'=4,'tp'=4] {'ep'}, dimensions={0}, use_global_device_ids=true | all-gather | bytes 327680 | tf_op jit(solution)/shard_map/all_gather | solution.py:15
  110.6 0.1 copy.37
  110.8 0.1 copy.36
  110.9 1.3 fusion.30
  112.2 20.3 %reduce-scatter.4.cloned.1.call-done = bf16[384,1024]{1,0:T(8,128)(2,1)} async-done(((bf16[1536,1024]{1,0:T(8,128)(2,1)}), bf16[384,1024]{1,0:T(8,128)(2,1)}) %reduce-scatter.4.cloned.1.call-update) | async-done | bytes 786448
  132.5 2.3 %copy.50 = bf16[384,1024]{0,1:T(8,128)(2,1)} copy(bf16[384,1024]{1,0:T(8,128)(2,1)} %reduce-scatter.4.cloned.1.call-done) | data formatting | bytes 1572864
  134.8 4.7 %all-to-all-start.1 = ((bf16[384,4,256]{0,2,1:T(8,128)(2,1)}), bf16[384,4,256]{0,2,1:T(8,128)(2,1)S(1)}, u32[]{:S(2)}, u32[]{:S(2)}) async-start(bf16[384,4,256]{0,2,1:T(8,128)(2,1)} %bitcast.87), calls=%async_computation.1 | async-start | bytes 1572864 | tf_op jit(solution)/shard_map/all_to_all | solution.py:92
  139.5 27.2 %all_gather.10 = bf16[512,256]{1,0:T(8,128)(2,1)S(1)} all-gather(bf16[128,256]{1,0:T(8,128)(2,1)S(1)} %copy-done.2), channel_id=1, replica_groups=mesh['grp'=2,'ep'=4,'tp'=4] {'ep'}, dimensions={0}, use_global_device_ids=true | all-gather | bytes 327680 | tf_op jit(solution)/shard_map/all_gather | solution.py:16
  166.7 0.9 copy.38
  167.6 1.5 fusion.11
  169.1 1.7 convolution_divide_fusion
  170.9 0.1 multiply_reduce_fusion
  171.0 0.1 multiply_convert_fusion.1
  171.1 0.7 copy.45
  171.8 1.9 %gather_fusion.1 = bf16[512,384]{1,0:T(8,128)(2,1)S(1)} fusion(bf16[384,1024]{0,1:T(8,128)(2,1)S(1)} %bitcast.85, s32[1024]{0:T(1024)S(1)} %pad_clamp_fusion), kind=kCustom, calls=%fused_computation.1 | custom fusion | bytes 788480 | tf_op jit(solution)/shard_map/jit(_take)/gather | solution.py:94
  173.8 0.1 gather.11
  173.9 1.7 fusion.15
  175.7 0.7 copy.55
  (31 shorter events, 0.1 us)
Async XLA Ops:
  7.2 78.6 %copy-start = (bf16[1,768,1536]{2,1,0:T(8,128)(2,1)S(1)}, bf16[1,768,1536]{2,1,0:T(8,128)(2,1)}, u32[]{:S(2)}) copy-start(bf16[1,768,1536]{2,1,0:T(8,128)(2,1)} %param.23) | copy-start | bytes 7077892
  7.2 70.3 %all-gather.2.cloned.1.call-start = ((), (), s32[]{:S(2)}) async-start(), calls=%async_computation.3 | async-start | bytes 3932160 | tf_op jit(solution)/shard_map/all_gather | solution.py:79
  49.7 82.8 %reduce-scatter.4.cloned.1.call-start = ((), (), s32[]{:S(2)}) async-start(), calls=%async_computation.4 | async-start | bytes 3932160
  77.4 5.4 %copy-start.8 = (bf16[4,256,1536]{2,1,0:T(8,128)(2,1)S(1)}, bf16[4,256,1536]{2,1,0:T(8,128)(2,1)}, u32[]{:S(2)}) copy-start(bf16[4,256,1536]{2,1,0:T(8,128)(2,1)} %all-gather.2.cloned.1.call-done) | copy-start | bytes 9437188
  77.4 5.4 %copy-start.9 = (bf16[1,1536,768]{2,1,0:T(8,128)(2,1)S(1)}, bf16[1,1536,768]{2,1,0:T(8,128)(2,1)}, u32[]{:S(2)}) copy-start(bf16[1,1536,768]{2,1,0:T(8,128)(2,1)} %param.21) | copy-start | bytes 7077892
  94.4 0.7 copy-start.4
  94.4 1.4 copy-start.5
  94.4 2.3 %copy-start.1 = (bf16[128,256]{1,0:T(8,128)(2,1)S(1)}, bf16[128,256]{1,0:T(8,128)(2,1)}, u32[]{:S(2)}) copy-start(bf16[128,256]{1,0:T(8,128)(2,1)} %param.13) | copy-start | bytes 196612
  94.4 16.4 %copy-start.3 = (bf16[128,256]{1,0:T(8,128)(2,1)S(1)}, bf16[128,256]{1,0:T(8,128)(2,1)}, u32[]{:S(2)}) copy-start(bf16[128,256]{1,0:T(8,128)(2,1)} %param.12) | copy-start | bytes 196612
  94.5 45.1 %copy-start.2 = (bf16[128,256]{1,0:T(8,128)(2,1)S(1)}, bf16[128,256]{1,0:T(8,128)(2,1)}, u32[]{:S(2)}) copy-start(bf16[128,256]{1,0:T(8,128)(2,1)} %param.14) | copy-start | bytes 196612
  112.2 58.6 %copy-start.6 = (f32[2]{0:T(128)S(1)}, f32[2]{0:T(128)}, u32[]{:S(2)}) copy-start(f32[2]{0:T(128)} %param.15) | copy-start | bytes 28
  134.8 36.2 %copy-start.7 = (f32[128]{0:T(128)S(1)}, f32[128]{0:T(128)}, u32[]{:S(2)}) copy-start(f32[128]{0:T(128)} %param.16) | copy-start | bytes 1540
  134.8 37.1 %all-to-all-start.1 = ((bf16[384,4,256]{0,2,1:T(8,128)(2,1)}), bf16[384,4,256]{0,2,1:T(8,128)(2,1)S(1)}, u32[]{:S(2)}, u32[]{:S(2)}) async-start(bf16[384,4,256]{0,2,1:T(8,128)(2,1)} %bitcast.87), calls=%async_computation.1 | async-start | bytes 1572864 | tf_op jit(solution)/shard_map/all_to_all | solution.py:92
Sparse Core Ops, SparseCore 0:
  49.8 27.5 all-gather.1
  94.6 37.8 reduce-scatter.3
where the time goes:
time: 184 us; the launch traced here: 183 us
  blocking collectives  67.5 us (37%)
  waiting for transfers between devices  48 us (26%)
  local copies, waits for them, and re-layouts  24.9 us (14%)
  matrix products  17 us (9%)
  between operations  14.3 us (8%)
  other arithmetic  6.72 us (4%)
  starting transfers between devices  4.81 us (3%)
    all_gather x1, waiting for transfers between devices, experts(): piece = lax.all_gather(arrived, 'tp', axis=2, tiled=True)  27.7 us
    all_gather x1, blocking collectives, attend(): value_piece = lax.all_gather(values, 'ep', axis=0, tiled=True)  27.2 us
    all_to_all x1, blocking collectives, experts(): lax.all_to_all(own_columns, 'ep', split_axis=0, concat_axis=0, tiled=True)  26.4 us
    unnamed x3, waiting for transfers between devices  20.3 us
    all_gather x1, blocking collectives, attend(): key_piece = lax.all_gather(keys, 'ep', axis=0, tiled=True)  13.9 us
    unnamed x26, local copies, waits for them, and re-layouts  10 us
    gather x1, local copies, waits for them, and re-layouts, experts(): outgoing = padded[owners].reshape(expert_count, capacity, width)  5.61 us
    dot_general x1, matrix products, experts(): jnp.einsum('scd,df->scf', piece, up_mat, preferred_element_type=jnp.float32)  5.36 us
  transfers between devices with their start and end apart: 3, of which 2 were waited for; matrix products, arithmetic and copies ran while one was open for 5% of the time, Pallas kernels for 0%

commit v1 on v0

--- a/solution.py
+++ b/solution.py
@@ -1,8 +1,15 @@
+import functools
+
 import jax
 import jax.numpy as jnp
 from jax import lax
+from jax.experimental import pallas as pl
+from jax.experimental.pallas import tpu as pltpu
 from jax.sharding import PartitionSpec as P
 
+MESH = pl.DeviceIdType.MESH
+F32 = jnp.float32
+BF16 = jnp.bfloat16
 
 def attend(queries, keys, values, lambdas, head_gain):
     row_count = queries.shape[0]
@@ -97,6 +104,381 @@
     return combined.astype(jnp.bfloat16)
 
 
+def visit_order(n):
+    return [sorted((s for s in range(n) if s != e), key=lambda s: (abs(s - e), s)) for e in range(n)]
+
+
+def fused_kernel(
+    n,
+    q_ref,
+    k_ref,
+    v_ref,
+    lam_ref,
+    hgain_ref,
+    tok_ref,
+    ids_ref,
+    rw_ref,
+    mgain_ref,
+    wg_hbm,
+    wu_hbm,
+    wd_hbm,
+    heads_ref,
+    out_ref,
+    wg,
+    wu,
+    wd,
+    gathered,
+    kbuf,
+    vbuf,
+    hid,
+    part,
+    core_in,
+    s_own,
+    s_out,
+    x_in,
+    t_out,
+    ret,
+    wsem,
+    own_send,
+    z_send,
+    z_recv,
+    x_send,
+    x_recv,
+    c_send,
+    c_recv,
+    kv_own,
+    kv_send,
+    kv_recv,
+    r1_send,
+    r1_recv,
+    r2_send,
+    r2_recv,
+    r3_send,
+    r3_recv,
+):
+    e = lax.axis_index("ep")
+    t = lax.axis_index("tp")
+    xi = t // 2
+    ci = lax.rem(t, 2)
+    core_peer = {"tp": 2 * xi + 1 - ci}
+    x_peer = {"tp": 2 * (1 - xi) + ci}
+    rows, width = tok_ref.shape
+    cols = width // 4
+    kv_rows = k_ref.shape[0]
+
+    def colblock(j):
+        return pl.ds(pl.multiple_of(j * cols, 128), cols)
+
+    def remote(src, dst, ss, rs, dev):
+        return pltpu.make_async_remote_copy(
+            src_ref=src, dst_ref=dst, send_sem=ss, recv_sem=rs, device_id=dev, device_id_type=MESH
+        )
+
+    weights = [
+        pltpu.make_async_copy(a, b, wsem.at[i])
+        for i, (a, b) in enumerate(((wg_hbm.at[0], wg), (wu_hbm.at[0], wu), (wd_hbm.at[0], wd)))
+    ]
+    for c in weights:
+        c.start()
+
+    barrier = pltpu.get_barrier_semaphore()
+    for d in range(1, n):
+        pl.semaphore_signal(barrier, inc=1, device_id={"ep": lax.rem(e + d, n)}, device_id_type=MESH)
+    pl.semaphore_signal(barrier, inc=1, device_id=core_peer, device_id_type=MESH)
+    pl.semaphore_signal(barrier, inc=1, device_id=x_peer, device_id_type=MESH)
+
+    step = 32
+
+    @pl.loop(0, rows // step)
+    def _(i):
+        sl = pl.ds(pl.multiple_of(i * step, step), step)
+        v = tok_ref[sl, :].astype(F32)
+        scale = lax.rsqrt(jnp.mean(v * v, axis=1, keepdims=True) + 1e-06)
+        gathered[e, sl, :] = (v * scale * mgain_ref[...]).astype(BF16)
+
+    pl.semaphore_wait(barrier, n + 1)
+
+    has_left = e > 0
+    has_right = e < n - 1
+    sides = ((0, has_left, e - 1), (1, has_right, e + 1))
+    own_tok = gathered.at[e, :, colblock(t)]
+    own_kv = pl.ds(pl.multiple_of(e * kv_rows, kv_rows), kv_rows)
+
+    def own_copies(side, peer):
+        dev = {"ep": peer}
+        return (
+            remote(own_tok, own_tok, own_send.at[side], z_recv.at[e], dev),
+            remote(k_ref, kbuf.at[own_kv], kv_own.at[0, side], kv_recv.at[0, e], dev),
+            remote(v_ref, vbuf.at[own_kv], kv_own.at[1, side], kv_recv.at[1, e], dev),
+        )
+
+    for side, has, peer in sides:
+
+        @pl.when(has)
+        def _():
+            for c in own_copies(side, peer):
+                c.start()
+
+    kbuf[own_kv, :] = k_ref[...]
+    vbuf[own_kv, :] = v_ref[...]
+
+    orders = visit_order(n)
+
+    def nth(k):
+        s = jnp.int32(orders[0][k])
+        for i in range(1, n):
+            s = jnp.where(e == i, jnp.int32(orders[i][k]), s)
+        return s
+
+    visits = [nth(k) for k in range(n - 1)]
+
+    def forward_of(s):
+        from_left = s < e
+        has = jnp.logical_or(
+            jnp.logical_and(from_left, has_right),
+            jnp.logical_and(jnp.logical_not(from_left), has_left),
+        )
+        return has, {"ep": jnp.clip(jnp.where(from_left, e + 1, e - 1), 0, n - 1)}
+
+    def z_copy(s):
+        blk = gathered.at[s, :, colblock(t)]
+        return remote(blk, blk, z_send.at[s], z_recv.at[s], forward_of(s)[1])
+
+    def x_copy(s):
+        blk = gathered.at[s, :, colblock(t)]
+        return remote(blk, blk, x_send.at[s], x_recv.at[s], x_peer)
+
+    def c_copy(s, which):
+        blk = gathered.at[s, :, colblock(t if which == 0 else 2 * (1 - xi) + ci)]
+        return remote(blk, blk, c_send.at[which, s], c_recv.at[which, s], core_peer)
+
+    def kv_copy(which, s):
+        sl = pl.ds(pl.multiple_of(s * kv_rows, kv_rows), kv_rows)
+        blk = (kbuf, vbuf)[which].at[sl]
+        return remote(blk, blk, kv_send.at[which, s], kv_recv.at[which, s], forward_of(s)[1])
+
+    def r1_copy(s, xx):
+        return remote(
+            part.at[s, :, colblock(2 * xx + 1 - ci)],
+            core_in.at[s, xx],
+            r1_send.at[xx, s],
+            r1_recv.at[xx, s],
+            core_peer,
+        )
+
+    def r2_copy(s):
+        return remote(s_out.at[s], x_in.at[s], r2_send.at[s], r2_recv.at[s], x_peer)
+
+    def r3_copy(s):
+        return remote(t_out.at[s], ret.at[e], r3_send.at[s], r3_recv.at[e], {"ep": s})
+
+    def ffn(s):
+        ff = wg.shape[1]
+        nb = 256
+
+        @pl.loop(0, ff // nb)
+        def _(b):
+            sl = pl.ds(pl.multiple_of(b * nb, nb), nb)
+            g = jnp.dot(gathered[s], wg[:, sl], preferred_element_type=F32)
+            u = jnp.dot(gathered[s], wu[:, sl], preferred_element_type=F32)
+            hid[:, sl] = (g / (1.0 + jnp.exp(-g)) * u).astype(BF16)
+
+        ob = 512
+
+        @pl.loop(0, width // ob)
+        def _(b):
+            sl = pl.ds(pl.multiple_of(b * ob, ob), ob)
+            part[s, :, sl] = jnp.dot(hid[...], wd[:, sl], preferred_element_type=F32).astype(BF16)
+
+        r1_copy(s, 1 - xi).start()
+        r1_copy(s, xi).start()
+
+    def reduce_core(s):
+        r1_copy(s, 1 - xi).wait_recv()
+        far = part[s, :, colblock(2 * (1 - xi) + ci)].astype(F32) + core_in[s, 1 - xi].astype(F32)
+        s_out[s] = far.astype(BF16)
+        r2_copy(s).start()
+        r1_copy(s, xi).wait_recv()
+        s_own[s] = part[s, :, colblock(t)].astype(F32) + core_in[s, xi].astype(F32)
+
+    def reduce_x(s):
+        r2_copy(s).wait_recv()
+        t_out[s] = (s_own[s] + x_in[s].astype(F32)).astype(BF16)
+
+        @pl.when(s != e)
+        def _():
+            r3_copy(s).start()
+
+    def arrive(s):
+        z_copy(s).wait_recv()
+
+        @pl.when(forward_of(s)[0])
+        def _():
+            z_copy(s).start()
+
+        x_copy(s).start()
+        c_copy(s, 0).start()
+
+    def relay_kv(s):
+        for w in (0, 1):
+            kv_copy(w, s).wait_recv()
+
+            @pl.when(forward_of(s)[0])
+            def _():
+                kv_copy(w, s).start()
+
+    def attend():
+        heads = lam_ref.shape[0]
+        vd = v_ref.shape[1] // heads
+        hd = q_ref.shape[1] // (2 * heads)
+        qr = q_ref.shape[0]
+        first = lax.broadcasted_iota(jnp.int32, (qr, 2 * hd), 1) < hd
+        for h in range(heads):
+            q = q_ref[:, h * 2 * hd : (h + 1) * 2 * hd].astype(F32)
+            both = jnp.concatenate(
+                [jnp.where(first, q, 0.0).astype(BF16), jnp.where(first, 0.0, q).astype(BF16)], axis=0
+            )
+            kh = kbuf[:, h * 2 * hd : (h + 1) * 2 * hd]
+            vh = vbuf[:, h * vd : (h + 1) * vd]
+            scores = lax.dot_general(
+                both, kh, (((1,), (1,)), ((), ())), preferred_element_type=F32
+            ) * (hd ** (-0.5))
+            ex = jnp.exp(scores - jnp.max(scores, axis=1, keepdims=True))
+            tot = jnp.sum(ex, axis=1, keepdims=True)
+            sums = jnp.dot(ex.astype(BF16), vh, preferred_element_type=F32) / tot
+            mixed = sums[:qr] - lam_ref[h] * sums[qr:]
+            norm = lax.rsqrt(jnp.mean(mixed * mixed, axis=1, keepdims=True) + 1e-06)
+            heads_ref[:, h * vd : (h + 1) * vd] = (mixed * norm * hgain_ref[...]).astype(BF16)
+
+    for c in weights:
+        c.wait()
+    ffn(e)
+    done = e
+    waiting = None
+    for s in visits:
+        arrive(s)
+        reduce_core(done)
+        x_copy(s).wait_recv()
+        c_copy(s, 1).start()
+        c_copy(s, 0).wait_recv()
+        c_copy(s, 1).wait_recv()
+        if waiting is not None:
+            reduce_x(waiting)
+        ffn(s)
+        relay_kv(s)
+        waiting, done = done, s
+    reduce_core(done)
+    reduce_x(waiting)
+    attend()
+    reduce_x(done)
+
+    total = None
+    ids = ids_ref[...]
+    rw = rw_ref[...]
+
+    def weight_of(x):
+        return jnp.sum(jnp.where(ids == x, rw, 0.0), axis=1, keepdims=True)
+
+    total = t_out[e].astype(F32) * weight_of(e)
+    for s in visits:
+        remote(t_out.at[s], ret.at[s], r3_send.at[s], r3_recv.at[s], {"ep": s}).wait_recv()
+        total = total + ret[s].astype(F32) * weight_of(s)
+    out_ref[...] = total.astype(BF16)
+
+    for side, has, peer in sides:
+
+        @pl.when(has)
+        def _():
+            for c in own_copies(side, peer):
+                c.wait_send()
+
+    for s in [e] + visits:
+        r1_copy(s, 1 - xi).wait_send()
+        r1_copy(s, xi).wait_send()
+        r2_copy(s).wait_send()
+    for s in visits:
+        x_copy(s).wait_send()
+        c_copy(s, 0).wait_send()
+        c_copy(s, 1).wait_send()
+        r3_copy(s).wait_send()
+
+        @pl.when(forward_of(s)[0])
+        def _():
+            z_copy(s).wait_send()
+            kv_copy(0, s).wait_send()
+            kv_copy(1, s).wait_send()
+
+
+def fused(queries, keys, values, lambdas, head_gain, tokens, route_ids, route_weights, moe_gain, w_gate, w_up, w_down):
+    n = lax.axis_size("ep")
+    rows, width = tokens.shape
+    cols = width // 4
+    ff = w_gate.shape[2]
+    vmem = pl.BlockSpec(memory_space=pltpu.VMEM)
+    smem = pl.BlockSpec(memory_space=pltpu.SMEM)
+    hbm = pl.BlockSpec(memory_space=pl.ANY)
+    dma = pltpu.SemaphoreType.DMA
+    return pl.pallas_call(
+        functools.partial(fused_kernel, n),
+        out_shape=(
+            jax.ShapeDtypeStruct((queries.shape[0], values.shape[1]), BF16),
+            jax.ShapeDtypeStruct((rows, cols), BF16),
+        ),
+        in_specs=[vmem, vmem, vmem, smem, vmem, vmem, vmem, vmem, vmem, hbm, hbm, hbm],
+        out_specs=(vmem, vmem),
+        scratch_shapes=[
+            pltpu.VMEM((width, ff), BF16),
+            pltpu.VMEM((width, ff), BF16),
+            pltpu.VMEM((ff, width), BF16),
+            pltpu.VMEM((n, rows, width), BF16),
+            pltpu.VMEM((n * keys.shape[0], keys.shape[1]), BF16),
+            pltpu.VMEM((n * values.shape[0], values.shape[1]), BF16),
+            pltpu.VMEM((rows, ff), BF16),
+            pltpu.VMEM((n, rows, width), BF16),
+            pltpu.VMEM((n, 2, rows, cols), BF16),
+            pltpu.VMEM((n, rows, cols), F32),
+            pltpu.VMEM((n, rows, cols), BF16),
+            pltpu.VMEM((n, rows, cols), BF16),
+            pltpu.VMEM((n, rows, cols), BF16),
+            pltpu.VMEM((n, rows, cols), BF16),
+            dma((3,)),
+            dma((2,)),
+            dma((n,)),
+            dma((n,)),
+            dma((n,)),
+            dma((n,)),
+            dma((2, n)),
+            dma((2, n)),
+            dma((2, 2)),
+            dma((2, n)),
+            dma((2, n)),
+            dma((2, n)),
+            dma((2, n)),
+            dma((n,)),
+            dma((n,)),
+            dma((n,)),
+            dma((n,)),
+        ],
+        compiler_params=pltpu.CompilerParams(
+            collective_id=0, has_side_effects=True, vmem_limit_bytes=60 * 1024 * 1024
+        ),
+        name="fused_layer",
+    )(
+        queries,
+        keys,
+        values,
+        lambdas,
+        head_gain.reshape(1, -1),
+        tokens,
+        route_ids,
+        route_weights,
+        moe_gain.reshape(1, -1),
+        w_gate,
+        w_up,
+        w_down,
+    )
+
+
 def on_device(
     queries,
     keys,
@@ -111,6 +493,14 @@
     w_up,
     w_down,
 ):
+    rows = tokens.shape[0]
+    expert_count = w_gate.shape[0] * lax.axis_size("ep")
+    slots = 2 * rows * route_ids.shape[1] // expert_count
+    if w_gate.shape[0] == 1 and lax.axis_size("tp") == 4 and slots >= rows:
+        return fused(
+            queries, keys, values, lambdas, head_gain, tokens,
+            route_ids, route_weights, moe_gain, w_gate, w_up, w_down,
+        )
     heads_out = attend(queries, keys, values, lambdas, head_gain)
     expert_out = experts(tokens, route_ids, route_weights, moe_gain, w_gate, w_up, w_down)
     return (heads_out, expert_out)

time: 184 us -> 74.1 us (0.40)
  blocking collectives: 67.5 us -> 0 us
  Pallas kernels: 0 us -> 65.8 us
  waiting for transfers between devices: 48 us -> 0 us
  local copies, waits for them, and re-layouts: 24.9 us -> 7.33 us
  matrix products: 17 us -> 0 us
  between operations: 14.3 us -> 0.64 us
  other arithmetic: 6.72 us -> 0 us
  starting transfers between devices: 4.81 us -> 0 us
    pallas_call x0 -> x1, Pallas kernels: none -> 65.8 us  [fused(): pl.pallas_call(functools.partial(fused_kernel, n), out_shape=(jax.ShapeDt...]
    all_gather x2 -> x0, blocking collectives: 41.2 us -> none  [the longest x1 27.2 us: attend(): value_piece = lax.all_gather(values, 'ep', axis=0, tiled=True)]
    all_gather x1 -> x0, waiting for transfers between devices: 27.7 us -> none  [experts(): piece = lax.all_gather(arrived, 'tp', axis=2, tiled=True)]
    all_to_all x1 -> x0, blocking collectives: 26.4 us -> none  [experts(): lax.all_to_all(own_columns, 'ep', split_axis=0, concat_axis=0, tiled=True)]
    unnamed x3 -> x0, waiting for transfers between devices: 20.3 us -> none
    dot_general x6 -> x0, matrix products: 17 us -> none  [the longest x1 5.36 us: experts(): jnp.einsum('scd,df->scf', piece, up_mat, preferred_element_type=jnp.float32)]
    gather x3 -> x0, local copies, waits for them, and re-layouts: 7.69 us -> none  [the longest x1 5.61 us: experts(): outgoing = padded[owners].reshape(expert_count, capacity, width)]
    all_to_all x1 -> x0, starting transfers between devices: 4.73 us -> none  [experts(): back = lax.all_to_all(summed, 'ep', split_axis=1, concat_axis=1, tiled=True)]
  transfers between devices with their start and end apart: 3 -> 0, of which waited for: 2 -> 0; matrix products, arithmetic and copies ran while one was open for 5% -> 0% of each run, Pallas kernels for 0% -> 0%
where the time goes in v1:
time: 74.1 us; the launch traced here: 73.8 us
  Pallas kernels  65.8 us (89%)
  local copies, waits for them, and re-layouts  7.33 us (10%)
    pallas_call x1, Pallas kernels, fused(): pl.pallas_call(functools.partial(fused_kernel, n), out_shape=(jax.ShapeDt...  65.8 us
    unnamed x4, local copies, waits for them, and re-layouts  6.04 us

profile of v1, /device:TPU:0, one launch (start us, length us, event | category | flops | bytes accessed | tf_op | source)
XLA Modules:
  0.0 73.8 jit_solution(4153775434255137282)
XLA Ops:
  0.6 1.3 %reshape.11.mgain_ref = f32[1,1536]{1,0:T(1,128)} reshape(f32[1536]{0:T(1024)} %param.20) | data formatting | bytes 12288 | tf_op jit(solution)/shard_map/reshape | solution.py:475
  1.9 1.5 %copy.14.ids_ref = s32[256,2]{1,0:T(8,128)} copy(s32[256,2]{0,1:T(2,128)} %param.18) | data formatting | bytes 4096 | tf_op args[6]
  3.4 1.5 %copy.15.rw_ref = f32[256,2]{1,0:T(8,128)} copy(f32[256,2]{0,1:T(2,128)} %param.19) | data formatting | bytes 4096 | tf_op args[7]
  4.9 65.8 %fused_layer.1 = (bf16[128,256]{1,0:T(8,128)(2,1)}, bf16[256,384]{1,0:T(8,128)(2,1)}) custom-call(bf16[128,256]{1,0:T(8,128)(2,1)} %q_ref.1, bf16[128,256]{1,0:T(8,128)(2,1)} %k_ref.1, bf16[128,256]{1,0:T(8,128)(2,1)} %v_ref.1, f32[2]{0:T(128)} %lam_ref.1, f32[1,128]{1,0:T(1,128)} %bitcast.1, bf16[256,1536]{1,0:T(8,128)(2,1)} %tok_ref.1, ...), custom_call_target="tpu_custom_call" | custom-call | tf_op jit(solution)/shard_map/fused_layer/pallas_call | solution.py:421
  70.7 1.5 %copy.18 = bf16[128,256]{1,0:T(8,128)(2,1)} copy(bf16[128,256]{1,0:T(8,128)(2,1)} %get-tuple-element.4) | data formatting | bytes 131072
  72.2 1.6 %copy.19 = bf16[256,384]{1,0:T(8,128)(2,1)} copy(bf16[256,384]{1,0:T(8,128)(2,1)} %get-tuple-element.5) | data formatting | bytes 393216

commit v2 on v1

--- a/solution.py
+++ b/solution.py
@@ -187,40 +187,37 @@
     pl.semaphore_signal(barrier, inc=1, device_id=core_peer, device_id_type=MESH)
     pl.semaphore_signal(barrier, inc=1, device_id=x_peer, device_id_type=MESH)
 
-    step = 32
-
-    @pl.loop(0, rows // step)
-    def _(i):
-        sl = pl.ds(pl.multiple_of(i * step, step), step)
-        v = tok_ref[sl, :].astype(F32)
-        scale = lax.rsqrt(jnp.mean(v * v, axis=1, keepdims=True) + 1e-06)
-        gathered[e, sl, :] = (v * scale * mgain_ref[...]).astype(BF16)
-
-    pl.semaphore_wait(barrier, n + 1)
+    halves = (0, 1)
+    hr = rows // 2
+
+    def half(h):
+        return pl.ds(h * hr, hr)
+
+    def normalize(h):
+        step = 32
+
+        @pl.loop(0, hr // step)
+        def _(i):
+            sl = pl.ds(pl.multiple_of(h * hr + i * step, step), step)
+            v = tok_ref[sl, :].astype(F32)
+            scale = lax.rsqrt(jnp.mean(v * v, axis=1, keepdims=True) + 1e-06)
+            gathered[e, sl, :] = (v * scale * mgain_ref[...]).astype(BF16)
 
     has_left = e > 0
     has_right = e < n - 1
     sides = ((0, has_left, e - 1), (1, has_right, e + 1))
-    own_tok = gathered.at[e, :, colblock(t)]
     own_kv = pl.ds(pl.multiple_of(e * kv_rows, kv_rows), kv_rows)
 
-    def own_copies(side, peer):
+    def own_tok(side, peer, h):
+        blk = gathered.at[e, half(h), colblock(t)]
+        return remote(blk, blk, own_send.at[side, h], z_recv.at[e, h], {"ep": peer})
+
+    def own_kv_copies(side, peer):
         dev = {"ep": peer}
         return (
-            remote(own_tok, own_tok, own_send.at[side], z_recv.at[e], dev),
             remote(k_ref, kbuf.at[own_kv], kv_own.at[0, side], kv_recv.at[0, e], dev),
             remote(v_ref, vbuf.at[own_kv], kv_own.at[1, side], kv_recv.at[1, e], dev),
         )
-
-    for side, has, peer in sides:
-
-        @pl.when(has)
-        def _():
-            for c in own_copies(side, peer):
-                c.start()
-
-    kbuf[own_kv, :] = k_ref[...]
-    vbuf[own_kv, :] = v_ref[...]
 
     orders = visit_order(n)
 
@@ -240,84 +237,103 @@
         )
         return has, {"ep": jnp.clip(jnp.where(from_left, e + 1, e - 1), 0, n - 1)}
 
-    def z_copy(s):
-        blk = gathered.at[s, :, colblock(t)]
-        return remote(blk, blk, z_send.at[s], z_recv.at[s], forward_of(s)[1])
-
-    def x_copy(s):
-        blk = gathered.at[s, :, colblock(t)]
-        return remote(blk, blk, x_send.at[s], x_recv.at[s], x_peer)
-
-    def c_copy(s, which):
-        blk = gathered.at[s, :, colblock(t if which == 0 else 2 * (1 - xi) + ci)]
-        return remote(blk, blk, c_send.at[which, s], c_recv.at[which, s], core_peer)
+    def z_copy(s, h):
+        blk = gathered.at[s, half(h), colblock(t)]
+        return remote(blk, blk, z_send.at[s, h], z_recv.at[s, h], forward_of(s)[1])
+
+    def x_copy(s, h):
+        blk = gathered.at[s, half(h), colblock(t)]
+        return remote(blk, blk, x_send.at[s, h], x_recv.at[s, h], x_peer)
+
+    def c_copy(s, h, which):
+        blk = gathered.at[s, half(h), colblock(t if which == 0 else 2 * (1 - xi) + ci)]
+        return remote(blk, blk, c_send.at[which, s, h], c_recv.at[which, s, h], core_peer)
 
     def kv_copy(which, s):
         sl = pl.ds(pl.multiple_of(s * kv_rows, kv_rows), kv_rows)
         blk = (kbuf, vbuf)[which].at[sl]
         return remote(blk, blk, kv_send.at[which, s], kv_recv.at[which, s], forward_of(s)[1])
 
-    def r1_copy(s, xx):
+    def r1_copy(s, h, xx):
         return remote(
-            part.at[s, :, colblock(2 * xx + 1 - ci)],
-            core_in.at[s, xx],
-            r1_send.at[xx, s],
-            r1_recv.at[xx, s],
+            part.at[s, half(h), colblock(2 * xx + 1 - ci)],
+            core_in.at[s, xx, half(h)],
+            r1_send.at[xx, s, h],
+            r1_recv.at[xx, s, h],
             core_peer,
         )
 
-    def r2_copy(s):
-        return remote(s_out.at[s], x_in.at[s], r2_send.at[s], r2_recv.at[s], x_peer)
-
-    def r3_copy(s):
-        return remote(t_out.at[s], ret.at[e], r3_send.at[s], r3_recv.at[e], {"ep": s})
-
-    def ffn(s):
-        ff = wg.shape[1]
-        nb = 256
-
-        @pl.loop(0, ff // nb)
-        def _(b):
-            sl = pl.ds(pl.multiple_of(b * nb, nb), nb)
-            g = jnp.dot(gathered[s], wg[:, sl], preferred_element_type=F32)
-            u = jnp.dot(gathered[s], wu[:, sl], preferred_element_type=F32)
-            hid[:, sl] = (g / (1.0 + jnp.exp(-g)) * u).astype(BF16)
-
-        ob = 512
-
-        @pl.loop(0, width // ob)
-        def _(b):
-            sl = pl.ds(pl.multiple_of(b * ob, ob), ob)
-            part[s, :, sl] = jnp.dot(hid[...], wd[:, sl], preferred_element_type=F32).astype(BF16)
-
-        r1_copy(s, 1 - xi).start()
-        r1_copy(s, xi).start()
+    def r2_copy(s, h):
+        return remote(
+            s_out.at[s, half(h)], x_in.at[s, half(h)], r2_send.at[s, h], r2_recv.at[s, h], x_peer
+        )
+
+    def r3_copy(s, h):
+        return remote(
+            t_out.at[s, half(h)],
+            ret.at[e, half(h)],
+            r3_send.at[s, h],
+            r3_recv.at[e, h],
+            {"ep": s},
+        )
+
+    ff = wg.shape[1]
+    nb = ff // 3
+    ob = width // 3
+
+    def up_step(s, b):
+        sl = pl.ds(b * nb, nb)
+        g = jnp.dot(gathered[s], wg[:, sl], preferred_element_type=F32)
+        u = jnp.dot(gathered[s], wu[:, sl], preferred_element_type=F32)
+        hid[:, sl] = (g / (1.0 + jnp.exp(-g)) * u).astype(BF16)
+
+    def down_step(s, b):
+        sl = pl.ds(b * ob, ob)
+        part[s, :, sl] = jnp.dot(hid[...], wd[:, sl], preferred_element_type=F32).astype(BF16)
+
+    def send_parts(s):
+        for h in halves:
+            r1_copy(s, h, 1 - xi).start()
+        for h in halves:
+            r1_copy(s, h, xi).start()
 
     def reduce_core(s):
-        r1_copy(s, 1 - xi).wait_recv()
-        far = part[s, :, colblock(2 * (1 - xi) + ci)].astype(F32) + core_in[s, 1 - xi].astype(F32)
-        s_out[s] = far.astype(BF16)
-        r2_copy(s).start()
-        r1_copy(s, xi).wait_recv()
+        for h in halves:
+            r1_copy(s, h, 1 - xi).wait_recv()
+            s_out[s, half(h)] = (
+                part[s, half(h), colblock(2 * (1 - xi) + ci)].astype(F32)
+                + core_in[s, 1 - xi, half(h)].astype(F32)
+            ).astype(BF16)
+            r2_copy(s, h).start()
+        for h in halves:
+            r1_copy(s, h, xi).wait_recv()
         s_own[s] = part[s, :, colblock(t)].astype(F32) + core_in[s, xi].astype(F32)
 
-    def reduce_x(s):
-        r2_copy(s).wait_recv()
-        t_out[s] = (s_own[s] + x_in[s].astype(F32)).astype(BF16)
-
-        @pl.when(s != e)
-        def _():
-            r3_copy(s).start()
-
-    def arrive(s):
-        z_copy(s).wait_recv()
+    def reduce_x(s, send=True):
+        for h in halves:
+            r2_copy(s, h).wait_recv()
+            t_out[s, half(h)] = (s_own[s, half(h)] + x_in[s, half(h)].astype(F32)).astype(BF16)
+            if send:
+                r3_copy(s, h).start()
+
+    def arrive(s, h):
+        z_copy(s, h).wait_recv()
 
         @pl.when(forward_of(s)[0])
         def _():
-            z_copy(s).start()
-
-        x_copy(s).start()
-        c_copy(s, 0).start()
+            z_copy(s, h).start()
+
+        x_copy(s, h).start()
+        c_copy(s, h, 0).start()
+
+    def cross(s, h):
+        x_copy(s, h).wait_recv()
+        c_copy(s, h, 1).start()
+
+    def ready(s):
+        for h in halves:
+            c_copy(s, h, 0).wait_recv()
+            c_copy(s, h, 1).wait_recv()
 
     def relay_kv(s):
         for w in (0, 1):
@@ -327,52 +343,103 @@
             def _():
                 kv_copy(w, s).start()
 
-    def attend():
+    def attend(h):
         heads = lam_ref.shape[0]
         vd = v_ref.shape[1] // heads
         hd = q_ref.shape[1] // (2 * heads)
         qr = q_ref.shape[0]
         first = lax.broadcasted_iota(jnp.int32, (qr, 2 * hd), 1) < hd
-        for h in range(heads):
-            q = q_ref[:, h * 2 * hd : (h + 1) * 2 * hd].astype(F32)
-            both = jnp.concatenate(
-                [jnp.where(first, q, 0.0).astype(BF16), jnp.where(first, 0.0, q).astype(BF16)], axis=0
-            )
-            kh = kbuf[:, h * 2 * hd : (h + 1) * 2 * hd]
-            vh = vbuf[:, h * vd : (h + 1) * vd]
-            scores = lax.dot_general(
-                both, kh, (((1,), (1,)), ((), ())), preferred_element_type=F32
-            ) * (hd ** (-0.5))
-            ex = jnp.exp(scores - jnp.max(scores, axis=1, keepdims=True))
-            tot = jnp.sum(ex, axis=1, keepdims=True)
-            sums = jnp.dot(ex.astype(BF16), vh, preferred_element_type=F32) / tot
-            mixed = sums[:qr] - lam_ref[h] * sums[qr:]
-            norm = lax.rsqrt(jnp.mean(mixed * mixed, axis=1, keepdims=True) + 1e-06)
-            heads_ref[:, h * vd : (h + 1) * vd] = (mixed * norm * hgain_ref[...]).astype(BF16)
-
+        q = q_ref[:, h * 2 * hd : (h + 1) * 2 * hd].astype(F32)
+        both = jnp.concatenate(
+            [jnp.where(first, q, 0.0).astype(BF16), jnp.where(first, 0.0, q).astype(BF16)], axis=0
+        )
+        kh = kbuf[:, h * 2 * hd : (h + 1) * 2 * hd]
+        vh = vbuf[:, h * vd : (h + 1) * vd]
+        scores = lax.dot_general(
+            both, kh, (((1,), (1,)), ((), ())), preferred_element_type=F32
+        ) * (hd ** (-0.5))
+        ex = jnp.exp(scores - jnp.max(scores, axis=1, keepdims=True))
+        tot = jnp.sum(ex, axis=1, keepdims=True)
+        sums = jnp.dot(ex.astype(BF16), vh, preferred_element_type=F32) / tot
+        mixed = sums[:qr] - lam_ref[h] * sums[qr:]
+        norm = lax.rsqrt(jnp.mean(mixed * mixed, axis=1, keepdims=True) + 1e-06)
+        heads_ref[:, h * vd : (h + 1) * vd] = (mixed * norm * hgain_ref[...]).astype(BF16)
+
+    for h in halves:
+        normalize(h)
+        if h == 0:
+            pl.semaphore_wait(barrier, n + 1)
+        for side, has, peer in sides:
+
+            @pl.when(has)
+            def _():
+                own_tok(side, peer, h).start()
+
+    kbuf[own_kv, :] = k_ref[...]
+    vbuf[own_kv, :] = v_ref[...]
+
+    def send_kv():
+        for side, has, peer in sides:
+
+            @pl.when(has)
+            def _():
+                for c in own_kv_copies(side, peer):
+                    c.start()
+
+    last = len(visits) - 1
     for c in weights:
         c.wait()
-    ffn(e)
-    done = e
-    waiting = None
-    for s in visits:
-        arrive(s)
-        reduce_core(done)
-        x_copy(s).wait_recv()
-        c_copy(s, 1).start()
-        c_copy(s, 0).wait_recv()
-        c_copy(s, 1).wait_recv()
-        if waiting is not None:
-            reduce_x(waiting)
-        ffn(s)
-        relay_kv(s)
-        waiting, done = done, s
-    reduce_core(done)
-    reduce_x(waiting)
-    attend()
-    reduce_x(done)
-
-    total = None
+    for b in range(3):
+        up_step(e, b)
+    for b in range(3):
+        down_step(e, b)
+    send_parts(e)
+    for h in halves:
+        arrive(visits[0], h)
+    for h in halves:
+        cross(visits[0], h)
+        if last >= 1:
+            arrive(visits[1], h)
+    ready(visits[0])
+    for k, s in enumerate(visits):
+        ahead = visits[k + 1] if k < last else None
+        further = visits[k + 2] if k + 1 < last else None
+        before = visits[k - 1] if k > 0 else None
+        up_step(s, 0)
+        if ahead is not None:
+            cross(ahead, 0)
+        if further is not None:
+            arrive(further, 0)
+        up_step(s, 1)
+        if ahead is not None:
+            cross(ahead, 1)
+        if further is not None:
+            arrive(further, 1)
+        if k == max(last - 2, 0):
+            send_kv()
+        up_step(s, 2)
+        if before is not None:
+            reduce_core(before)
+            relay_kv(before)
+        for b in range(3):
+            down_step(s, b)
+        send_parts(s)
+        if ahead is not None:
+            ready(ahead)
+    for k in range(max(last - 1, 0)):
+        reduce_x(visits[k])
+    reduce_core(visits[last])
+    reduce_core(e)
+    relay_kv(visits[last])
+    heads = lam_ref.shape[0]
+    attend(0)
+    if last >= 1:
+        reduce_x(visits[last - 1])
+    for h in range(1, heads):
+        attend(h)
+    reduce_x(visits[last])
+    reduce_x(e, send=False)
+
     ids = ids_ref[...]
     rw = rw_ref[...]
 
@@ -381,7 +448,14 @@
 
     total = t_out[e].astype(F32) * weight_of(e)
     for s in visits:
-        remote(t_out.at[s], ret.at[s], r3_send.at[s], r3_recv.at[s], {"ep": s}).wait_recv()
+        for h in halves:
+            remote(
+                t_out.at[s, half(h)],
+                ret.at[s, half(h)],
+                r3_send.at[s, h],
+                r3_recv.at[s, h],
+                {"ep": s},
+            ).wait_recv()
         total = total + ret[s].astype(F32) * weight_of(s)
     out_ref[...] = total.astype(BF16)
 
@@ -389,22 +463,27 @@
 
         @pl.when(has)
         def _():
-            for c in own_copies(side, peer):
+            for h in halves:
+                own_tok(side, peer, h).wait_send()
+            for c in own_kv_copies(side, peer):
                 c.wait_send()
 
     for s in [e] + visits:
-        r1_copy(s, 1 - xi).wait_send()
-        r1_copy(s, xi).wait_send()
-        r2_copy(s).wait_send()
+        for h in halves:
+            r1_copy(s, h, 1 - xi).wait_send()
+            r1_copy(s, h, xi).wait_send()
+            r2_copy(s, h).wait_send()
     for s in visits:
-        x_copy(s).wait_send()
-        c_copy(s, 0).wait_send()
-        c_copy(s, 1).wait_send()
-        r3_copy(s).wait_send()
+        for h in halves:
+            x_copy(s, h).wait_send()
+            c_copy(s, h, 0).wait_send()
+            c_copy(s, h, 1).wait_send()
+            r3_copy(s, h).wait_send()
 
         @pl.when(forward_of(s)[0])
         def _():
-            z_copy(s).wait_send()
+            for h in halves:
+                z_copy(s, h).wait_send()
             kv_copy(0, s).wait_send()
             kv_copy(1, s).wait_send()
 
@@ -442,22 +521,22 @@
             pltpu.VMEM((n, rows, cols), BF16),
             pltpu.VMEM((n, rows, cols), BF16),
             dma((3,)),
-            dma((2,)),
-            dma((n,)),
-            dma((n,)),
-            dma((n,)),
-            dma((n,)),
-            dma((2, n)),
-            dma((2, n)),
+            dma((2, 2)),
+            dma((n, 2)),
+            dma((n, 2)),
+            dma((n, 2)),
+            dma((n, 2)),
+            dma((2, n, 2)),
+            dma((2, n, 2)),
             dma((2, 2)),
             dma((2, n)),
             dma((2, n)),
-            dma((2, n)),
-            dma((2, n)),
-            dma((n,)),
-            dma((n,)),
-            dma((n,)),
-            dma((n,)),
+            dma((2, n, 2)),
+            dma((2, n, 2)),
+            dma((n, 2)),
+            dma((n, 2)),
+            dma((n, 2)),
+            dma((n, 2)),
         ],
         compiler_params=pltpu.CompilerParams(
             collective_id=0, has_side_effects=True, vmem_limit_bytes=60 * 1024 * 1024

time: 74.1 us -> 72.9 us (0.984)
  Pallas kernels: 65.8 us -> 64.6 us
    pallas_call x1, Pallas kernels: 65.8 us -> 64.6 us  [fused(): pl.pallas_call(functools.partial(fused_kernel, n), out_shape=(jax.ShapeDt...]
where the time goes in v2:
time: 72.9 us; the launch traced here: 72.6 us
  Pallas kernels  64.6 us (89%)
  local copies, waits for them, and re-layouts  7.33 us (10%)
    pallas_call x1, Pallas kernels, fused(): pl.pallas_call(functools.partial(fused_kernel, n), out_shape=(jax.ShapeDt...  64.6 us
    unnamed x4, local copies, waits for them, and re-layouts  6.04 us

profile of v2, /device:TPU:0, one launch (start us, length us, event | category | flops | bytes accessed | tf_op | source)
XLA Modules:
  0.0 72.6 jit_solution(17528577654902183594)
XLA Ops:
  0.6 1.3 %reshape.11.mgain_ref = f32[1,1536]{1,0:T(1,128)} reshape(f32[1536]{0:T(1024)} %param.20) | data formatting | bytes 12288 | tf_op jit(solution)/shard_map/reshape | solution.py:554
  1.9 1.5 %copy.14.ids_ref = s32[256,2]{1,0:T(8,128)} copy(s32[256,2]{0,1:T(2,128)} %param.18) | data formatting | bytes 4096 | tf_op args[6]
  3.4 1.5 %copy.15.rw_ref = f32[256,2]{1,0:T(8,128)} copy(f32[256,2]{0,1:T(2,128)} %param.19) | data formatting | bytes 4096 | tf_op args[7]
  4.9 64.6 %fused_layer.1 = (bf16[128,256]{1,0:T(8,128)(2,1)}, bf16[256,384]{1,0:T(8,128)(2,1)}) custom-call(bf16[128,256]{1,0:T(8,128)(2,1)} %q_ref.1, bf16[128,256]{1,0:T(8,128)(2,1)} %k_ref.1, bf16[128,256]{1,0:T(8,128)(2,1)} %v_ref.1, f32[2]{0:T(128)} %lam_ref.1, f32[1,128]{1,0:T(1,128)} %bitcast.1, bf16[256,1536]{1,0:T(8,128)(2,1)} %tok_ref.1, ...), custom_call_target="tpu_custom_call" | custom-call | tf_op jit(solution)/shard_map/fused_layer/pallas_call | solution.py:500
  69.5 1.5 %copy.18 = bf16[128,256]{1,0:T(8,128)(2,1)} copy(bf16[128,256]{1,0:T(8,128)(2,1)} %get-tuple-element.4) | data formatting | bytes 131072
  70.9 1.6 %copy.19 = bf16[256,384]{1,0:T(8,128)(2,1)} copy(bf16[256,384]{1,0:T(8,128)(2,1)} %get-tuple-element.5) | data formatting | bytes 393216

commit v3 on v2

--- a/solution.py
+++ b/solution.py
@@ -138,6 +138,7 @@
     x_in,
     t_out,
     ret,
+    out_weights,
     wsem,
     own_send,
     z_send,
@@ -146,7 +147,6 @@
     x_recv,
     c_send,
     c_recv,
-    kv_own,
     kv_send,
     kv_recv,
     r1_send,
@@ -212,11 +212,18 @@
         blk = gathered.at[e, half(h), colblock(t)]
         return remote(blk, blk, own_send.at[side, h], z_recv.at[e, h], {"ep": peer})
 
-    def own_kv_copies(side, peer):
-        dev = {"ep": peer}
+    def kv_copies(s):
+        dev = {"ep": s}
         return (
-            remote(k_ref, kbuf.at[own_kv], kv_own.at[0, side], kv_recv.at[0, e], dev),
-            remote(v_ref, vbuf.at[own_kv], kv_own.at[1, side], kv_recv.at[1, e], dev),
+            remote(k_ref, kbuf.at[own_kv], kv_send.at[0, s], kv_recv.at[0, e], dev),
+            remote(v_ref, vbuf.at[own_kv], kv_send.at[1, s], kv_recv.at[1, e], dev),
+        )
+
+    def kv_arrivals(s):
+        sl = pl.ds(pl.multiple_of(s * kv_rows, kv_rows), kv_rows)
+        return (
+            remote(k_ref, kbuf.at[sl], kv_send.at[0, s], kv_recv.at[0, s], {"ep": s}),
+            remote(v_ref, vbuf.at[sl], kv_send.at[1, s], kv_recv.at[1, s], {"ep": s}),
         )
 
     orders = visit_order(n)
@@ -248,11 +255,6 @@
     def c_copy(s, h, which):
         blk = gathered.at[s, half(h), colblock(t if which == 0 else 2 * (1 - xi) + ci)]
         return remote(blk, blk, c_send.at[which, s, h], c_recv.at[which, s, h], core_peer)
-
-    def kv_copy(which, s):
-        sl = pl.ds(pl.multiple_of(s * kv_rows, kv_rows), kv_rows)
-        blk = (kbuf, vbuf)[which].at[sl]
-        return remote(blk, blk, kv_send.at[which, s], kv_recv.at[which, s], forward_of(s)[1])
 
     def r1_copy(s, h, xx):
         return remote(
@@ -334,14 +336,6 @@
         for h in halves:
             c_copy(s, h, 0).wait_recv()
             c_copy(s, h, 1).wait_recv()
-
-    def relay_kv(s):
-        for w in (0, 1):
-            kv_copy(w, s).wait_recv()
-
-            @pl.when(forward_of(s)[0])
-            def _():
-                kv_copy(w, s).start()
 
     def attend(h):
         heads = lam_ref.shape[0]
@@ -379,12 +373,16 @@
     vbuf[own_kv, :] = v_ref[...]
 
     def send_kv():
-        for side, has, peer in sides:
-
-            @pl.when(has)
-            def _():
-                for c in own_kv_copies(side, peer):
-                    c.start()
+        for s in visits:
+            for c in kv_copies(s):
+                c.start()
+
+    ids = ids_ref[...]
+    rw = rw_ref[...]
+    lines = [jnp.sum(jnp.where(ids == x, rw, 0.0), axis=0, keepdims=True) for x in [e] + visits]
+    pad = (-len(lines)) % 8
+    lines.append(jnp.zeros((pad, rows), F32))
+    out_weights[...] = jnp.concatenate(lines, axis=0).T
 
     last = len(visits) - 1
     for c in weights:
@@ -420,7 +418,6 @@
         up_step(s, 2)
         if before is not None:
             reduce_core(before)
-            relay_kv(before)
         for b in range(3):
             down_step(s, b)
         send_parts(s)
@@ -430,8 +427,10 @@
         reduce_x(visits[k])
     reduce_core(visits[last])
     reduce_core(e)
-    relay_kv(visits[last])
     heads = lam_ref.shape[0]
+    for s in visits:
+        for c in kv_arrivals(s):
+            c.wait_recv()
     attend(0)
     if last >= 1:
         reduce_x(visits[last - 1])
@@ -440,14 +439,8 @@
     reduce_x(visits[last])
     reduce_x(e, send=False)
 
-    ids = ids_ref[...]
-    rw = rw_ref[...]
-
-    def weight_of(x):
-        return jnp.sum(jnp.where(ids == x, rw, 0.0), axis=1, keepdims=True)
-
-    total = t_out[e].astype(F32) * weight_of(e)
-    for s in visits:
+    total = out_weights[:, 0:1] * t_out[e].astype(F32)
+    for k, s in enumerate(visits):
         for h in halves:
             remote(
                 t_out.at[s, half(h)],
@@ -456,7 +449,7 @@
                 r3_recv.at[s, h],
                 {"ep": s},
             ).wait_recv()
-        total = total + ret[s].astype(F32) * weight_of(s)
+        total = total + ret[s].astype(F32) * out_weights[:, k + 1 : k + 2]
     out_ref[...] = total.astype(BF16)
 
     for side, has, peer in sides:
@@ -465,8 +458,6 @@
         def _():
             for h in halves:
                 own_tok(side, peer, h).wait_send()
-            for c in own_kv_copies(side, peer):
-                c.wait_send()
 
     for s in [e] + visits:
         for h in halves:
@@ -479,13 +470,18 @@
             c_copy(s, h, 0).wait_send()
             c_copy(s, h, 1).wait_send()
             r3_copy(s, h).wait_send()
+        for c in kv_copies(s):
+            c.wait_send()
 
         @pl.when(forward_of(s)[0])
         def _():
             for h in halves:
                 z_copy(s, h).wait_send()
-            kv_copy(0, s).wait_send()
-            kv_copy(1, s).wait_send()
+
+
+def hand_on_kernel(a_ref, b_ref, c_ref, d_ref):
+    c_ref[...] = a_ref[...]
+    d_ref[...] = b_ref[...]
 
 
 def fused(queries, keys, values, lambdas, head_gain, tokens, route_ids, route_weights, moe_gain, w_gate, w_up, w_down):
@@ -497,7 +493,7 @@
     smem = pl.BlockSpec(memory_space=pltpu.SMEM)
     hbm = pl.BlockSpec(memory_space=pl.ANY)
     dma = pltpu.SemaphoreType.DMA
-    return pl.pallas_call(
+    results = pl.pallas_call(
         functools.partial(fused_kernel, n),
         out_shape=(
             jax.ShapeDtypeStruct((queries.shape[0], values.shape[1]), BF16),
@@ -520,6 +516,7 @@
             pltpu.VMEM((n, rows, cols), BF16),
             pltpu.VMEM((n, rows, cols), BF16),
             pltpu.VMEM((n, rows, cols), BF16),
+            pltpu.VMEM((rows, -(-n // 8) * 8), F32),
             dma((3,)),
             dma((2, 2)),
             dma((n, 2)),
@@ -528,7 +525,6 @@
             dma((n, 2)),
             dma((2, n, 2)),
             dma((2, n, 2)),
-            dma((2, 2)),
             dma((2, n)),
             dma((2, n)),
             dma((2, n, 2)),
@@ -547,15 +543,22 @@
         keys,
         values,
         lambdas,
-        head_gain.reshape(1, -1),
+        head_gain,
         tokens,
-        route_ids,
-        route_weights,
-        moe_gain.reshape(1, -1),
+        route_ids.T,
+        route_weights.T,
+        moe_gain,
         w_gate,
         w_up,
         w_down,
     )
+    return pl.pallas_call(
+        hand_on_kernel,
+        out_shape=tuple(jax.ShapeDtypeStruct(r.shape, r.dtype) for r in results),
+        in_specs=[vmem, vmem],
+        out_specs=(vmem, vmem),
+        name="hand_on",
+    )(*results)
 
 
 def on_device(

time: 72.9 us -> 58.9 us (0.81)
  local copies, waits for them, and re-layouts: 7.33 us -> 0 us
  Pallas kernels: 64.6 us -> 58 us
    pallas_call x1, Pallas kernels: 64.6 us -> 56.4 us  [fused(): pl.pallas_call(functools.partial(fused_kernel, n), out_shape=(jax.ShapeDt...]
    unnamed x4 -> x0, local copies, waits for them, and re-layouts: 6.04 us -> none
    pallas_call x0 -> x1, Pallas kernels: none -> 1.67 us  [fused(): pl.pallas_call(hand_on_kernel, out_shape=tuple((jax.ShapeDtypeStruct(r.sh...]
    reshape x1 -> x0, local copies, waits for them, and re-layouts: 1.29 us -> none  [fused(): moe_gain.reshape(1, -1)]
where the time goes in v3:
time: 58.9 us; the launch traced here: 58.7 us
  Pallas kernels  58 us (98%)
  between operations  0.64 us (1%)
    pallas_call x1, Pallas kernels, fused(): pl.pallas_call(functools.partial(fused_kernel, n), out_shape=(jax.ShapeDt...  56.4 us
    pallas_call x1, Pallas kernels, fused(): pl.pallas_call(hand_on_kernel, out_shape=tuple((jax.ShapeDtypeStruct(r.sh...  1.67 us

profile of v3, /device:TPU:0, one launch (start us, length us, event | category | flops | bytes accessed | tf_op | source)
XLA Modules:
  0.0 58.7 jit_solution(17806928609346483035)
XLA Ops:
  0.6 56.4 %fused_layer.1 = (bf16[128,256]{1,0:T(8,128)(2,1)}, bf16[256,384]{1,0:T(8,128)(2,1)}) custom-call(bf16[128,256]{1,0:T(8,128)(2,1)} %q_ref.1, bf16[128,256]{1,0:T(8,128)(2,1)} %k_ref.1, bf16[128,256]{1,0:T(8,128)(2,1)} %v_ref.1, f32[2]{0:T(128)} %lam_ref.1, f32[128]{0:T(128)} %hgain_ref.1, bf16[256,1536]{1,0:T(8,128)(2,1)} %tok_ref.1, s32[2,256]{1,0:T(2,128)} %bitcast.2, ...), custom_call_target="tpu_custom_call" | custom-call | tf_op jit(solution)/shard_map/fused_layer/pallas_call | solution.py:496
  57.0 1.7 %hand_on.1 = (bf16[128,256]{1,0:T(8,128)(2,1)}, bf16[256,384]{1,0:T(8,128)(2,1)}) custom-call(bf16[128,256]{1,0:T(8,128)(2,1)} %get-tuple-element.4.a_ref, bf16[256,384]{1,0:T(8,128)(2,1)} %get-tuple-element.5.b_ref), custom_call_target="tpu_custom_call" | custom-call | tf_op jit(solution)/shard_map/hand_on/pallas_call | solution.py:555

commit v4 on v3

--- a/solution.py
+++ b/solution.py
@@ -10,6 +10,7 @@
 MESH = pl.DeviceIdType.MESH
 F32 = jnp.float32
 BF16 = jnp.bfloat16
+PIECES = 2
 
 def attend(queries, keys, values, lambdas, head_gain):
     row_count = queries.shape[0]
@@ -187,8 +188,8 @@
     pl.semaphore_signal(barrier, inc=1, device_id=core_peer, device_id_type=MESH)
     pl.semaphore_signal(barrier, inc=1, device_id=x_peer, device_id_type=MESH)
 
-    halves = (0, 1)
-    hr = rows // 2
+    halves = range(PIECES)
+    hr = rows // PIECES
 
     def half(h):
         return pl.ds(h * hr, hr)
@@ -281,7 +282,6 @@
 
     ff = wg.shape[1]
     nb = ff // 3
-    ob = width // 3
 
     def up_step(s, b):
         sl = pl.ds(b * nb, nb)
@@ -289,15 +289,17 @@
         u = jnp.dot(gathered[s], wu[:, sl], preferred_element_type=F32)
         hid[:, sl] = (g / (1.0 + jnp.exp(-g)) * u).astype(BF16)
 
-    def down_step(s, b):
-        sl = pl.ds(b * ob, ob)
+    def down_step(s, j):
+        sl = colblock(j)
         part[s, :, sl] = jnp.dot(hid[...], wd[:, sl], preferred_element_type=F32).astype(BF16)
 
-    def send_parts(s):
-        for h in halves:
-            r1_copy(s, h, 1 - xi).start()
-        for h in halves:
-            r1_copy(s, h, xi).start()
+    def down(s):
+        for xx in (1 - xi, xi):
+            down_step(s, 2 * xx + 1 - ci)
+            for h in halves:
+                r1_copy(s, h, xx).start()
+        for xx in (1 - xi, xi):
+            down_step(s, 2 * xx + ci)
 
     def reduce_core(s):
         for h in halves:
@@ -318,15 +320,20 @@
             if send:
                 r3_copy(s, h).start()
 
-    def arrive(s, h):
+    def take(s, h):
         z_copy(s, h).wait_recv()
 
         @pl.when(forward_of(s)[0])
         def _():
             z_copy(s, h).start()
 
+    def share(s, h):
         x_copy(s, h).start()
         c_copy(s, h, 0).start()
+
+    def arrive(s, h):
+        take(s, h)
+        share(s, h)
 
     def cross(s, h):
         x_copy(s, h).wait_recv()
@@ -389,38 +396,59 @@
         c.wait()
     for b in range(3):
         up_step(e, b)
-    for b in range(3):
-        down_step(e, b)
-    send_parts(e)
-    for h in halves:
-        arrive(visits[0], h)
-    for h in halves:
-        cross(visits[0], h)
+    down(e)
+    inner = jnp.logical_and(has_left, has_right)
+    outer = jnp.logical_not(inner)
+
+    @pl.when(inner)
+    def _():
+        for h in halves:
+            arrive(visits[0], h)
+            if last >= 1:
+                take(visits[1], h)
         if last >= 1:
-            arrive(visits[1], h)
+            for h in halves:
+                share(visits[1], h)
+        for h in halves:
+            cross(visits[0], h)
+        if last >= 2:
+            for h in halves:
+                arrive(visits[2], h)
+
+    @pl.when(outer)
+    def _():
+        for h in halves:
+            arrive(visits[0], h)
+        for h in halves:
+            cross(visits[0], h)
+            if last >= 1:
+                arrive(visits[1], h)
+
     ready(visits[0])
     for k, s in enumerate(visits):
         ahead = visits[k + 1] if k < last else None
         further = visits[k + 2] if k + 1 < last else None
         before = visits[k - 1] if k > 0 else None
-        up_step(s, 0)
-        if ahead is not None:
-            cross(ahead, 0)
-        if further is not None:
-            arrive(further, 0)
-        up_step(s, 1)
-        if ahead is not None:
-            cross(ahead, 1)
-        if further is not None:
-            arrive(further, 1)
+        for b, group in enumerate((halves[: PIECES // 2], halves[PIECES // 2 :])):
+            up_step(s, b)
+            for h in group:
+                if ahead is not None:
+                    cross(ahead, h)
+                if further is not None:
+                    if k == 0:
+
+                        @pl.when(outer)
+                        def _():
+                            arrive(further, h)
+
+                    else:
+                        arrive(further, h)
         if k == max(last - 2, 0):
             send_kv()
-        up_step(s, 2)
         if before is not None:
             reduce_core(before)
-        for b in range(3):
-            down_step(s, b)
-        send_parts(s)
+        up_step(s, 2)
+        down(s)
         if ahead is not None:
             ready(ahead)
     for k in range(max(last - 1, 0)):
@@ -518,21 +546,21 @@
             pltpu.VMEM((n, rows, cols), BF16),
             pltpu.VMEM((rows, -(-n // 8) * 8), F32),
             dma((3,)),
-            dma((2, 2)),
-            dma((n, 2)),
-            dma((n, 2)),
-            dma((n, 2)),
-            dma((n, 2)),
-            dma((2, n, 2)),
-            dma((2, n, 2)),
+            dma((2, PIECES)),
+            dma((n, PIECES)),
+            dma((n, PIECES)),
+            dma((n, PIECES)),
+            dma((n, PIECES)),
+            dma((2, n, PIECES)),
+            dma((2, n, PIECES)),
             dma((2, n)),
             dma((2, n)),
-            dma((2, n, 2)),
-            dma((2, n, 2)),
-            dma((n, 2)),
-            dma((n, 2)),
-            dma((n, 2)),
-            dma((n, 2)),
+            dma((2, n, PIECES)),
+            dma((2, n, PIECES)),
+            dma((n, PIECES)),
+            dma((n, PIECES)),
+            dma((n, PIECES)),
+            dma((n, PIECES)),
         ],
         compiler_params=pltpu.CompilerParams(
             collective_id=0, has_side_effects=True, vmem_limit_bytes=60 * 1024 * 1024

time: 58.9 us -> 55.5 us (0.942)
  Pallas kernels: 58 us -> 54.7 us
    pallas_call x1, Pallas kernels: 56.4 us -> 53.1 us  [fused(): pl.pallas_call(functools.partial(fused_kernel, n), out_shape=(jax.ShapeDt...]
where the time goes in v4:
time: 55.5 us; the launch traced here: 55.4 us
  Pallas kernels  54.7 us (99%)
  between operations  0.64 us (1%)
    pallas_call x1, Pallas kernels, fused(): pl.pallas_call(functools.partial(fused_kernel, n), out_shape=(jax.ShapeDt...  53.1 us
    pallas_call x1, Pallas kernels, fused(): pl.pallas_call(hand_on_kernel, out_shape=tuple((jax.ShapeDtypeStruct(r.sh...  1.67 us

profile of v4, /device:TPU:0, one launch (start us, length us, event | category | flops | bytes accessed | tf_op | source)
XLA Modules:
  0.0 55.4 jit_solution(15053745430539916427)
XLA Ops:
  0.6 53.1 %fused_layer.1 = (bf16[128,256]{1,0:T(8,128)(2,1)}, bf16[256,384]{1,0:T(8,128)(2,1)}) custom-call(bf16[128,256]{1,0:T(8,128)(2,1)} %q_ref.1, bf16[128,256]{1,0:T(8,128)(2,1)} %k_ref.1, bf16[128,256]{1,0:T(8,128)(2,1)} %v_ref.1, f32[2]{0:T(128)} %lam_ref.1, f32[128]{0:T(128)} %hgain_ref.1, bf16[256,1536]{1,0:T(8,128)(2,1)} %tok_ref.1, s32[2,256]{1,0:T(2,128)} %bitcast.2, ...), custom_call_target="tpu_custom_call" | custom-call | tf_op jit(solution)/shard_map/fused_layer/pallas_call | solution.py:524
  53.7 1.7 %hand_on.1 = (bf16[128,256]{1,0:T(8,128)(2,1)}, bf16[256,384]{1,0:T(8,128)(2,1)}) custom-call(bf16[128,256]{1,0:T(8,128)(2,1)} %get-tuple-element.4.a_ref, bf16[256,384]{1,0:T(8,128)(2,1)} %get-tuple-element.5.b_ref), custom_call_target="tpu_custom_call" | custom-call | tf_op jit(solution)/shard_map/hand_on/pallas_call | solution.py:583
